TPU v7x, 32 devices: a whole 2x2x4 slice. The times are simulated.
32 devices in a mesh: sp: 8 (over z, x), tp: 4 (over y, core).
Axes of the slice: x: 2, y: 2, z: 4, core: 2. Of those that a mesh axis runs over, the one named last changes fastest.
Arguments:
- grid_in: bfloat16 [1024, 2048], P('sp', 'tp'), may hold values from -6 to 6
- documents: int32 [1024], P('sp'), may hold values from 0 to 3, never falling along the last dimension, each value on 1 to 512 neighbouring positions
- pre_gain: float32 [2, 2048], replicated, may hold values from 0.1 to 1.9
- query_weight: bfloat16 [2, 2048, 2048], P(None, None, 'tp'), may hold values from -1 to 1
- key_weight: bfloat16 [2, 2048, 2048], P(None, None, 'tp'), may hold values from -4 to 4
- value_weight: bfloat16 [2, 2048, 2048], P(None, None, 'tp'), may hold values from -0.125 to 0.125
- offset_bias: float32 [2, 32, 15, 31], P(None, 'tp'), may hold values from -5 to 5
- out_weight: bfloat16 [2, 2048, 2048], P(None, None, 'tp'), may hold values from -3 to 3
- post_gain: float32 [2, 2048], P(None, 'tp'), may hold values from 0.1 to 1.9
Outputs:
- grid_out: bfloat16 [1024, 2048], P('sp', 'tp')
Inputs may be any that keep to these rules, and one draw needn't show every extreme that they name: `documents`: each position's document number; numbers never fall along the token order, and each document covers 1 to 512 positions.
All inputs are finite; a program needn't handle non-finite values.
Results may differ from a plain program's by a relative error of at most 0.0095.
Values may be sent and summed in bfloat16 or wider, within the bound.
A program may use at most 64 MiB of HBM per device.

v0:
```python
import functools

import jax
import jax.numpy as jnp
from jax import lax
from jax.experimental import pallas as pl
from jax.experimental.pallas import tpu as pltpu
from jax.sharding import PartitionSpec as P

HEAD_DIM = 64
WIN_ROWS = 8
WIN_COLS = 16
GRID_W = 32
LAYERS = 2
EPS = 1e-06
MESH = pl.DeviceIdType.MESH
F32 = jnp.float32
BF16 = jnp.bfloat16


def kernel(
    nsp, ntp, heads, chunks, x_hbm, doc_hbm, pre_hbm, ob_hbm, post_hbm, wq_hbm, wk_hbm, wv_hbm, wo_hbm,
    upd_ref, stream_ref,
    xg, bg, att, docs, pg, ssq, w_all, xs, qb, kb, vb, mask, bias, fb, doc_ref, pre_ref, ob_ref,
    w_sem, loc_sem, sp_s, sp_r, y_s, y_r, p_s, p_r, ay_s, ay_r, ap_s, ap_r, d_s, d_r, g_s, g_r, q_s, q_r,
):
    s = lax.axis_index("sp")
    t = lax.axis_index("tp")
    nc = ntp // 2
    n, feat = x_hbm.shape
    width = feat * ntp
    keys = 3 * n
    pairs = heads // 2
    row_count = n // GRID_W
    rim = WIN_ROWS // 2
    core = lax.rem(t, 2)
    partner = t + 1 - 2 * core
    odd = lax.rem(s, 2)
    step = 1 - 2 * odd
    s_near = s + step
    near_row = 2 - 2 * odd
    far_row = 2 * odd
    up = s + 2 * step
    has_up = (up >= 0) & (up < nsp)
    down = s - 2 * step
    has_far = (down >= 0) & (down < nsp)
    s_up = jnp.clip(up, 0, nsp - 1)
    s_down = jnp.clip(down, 0, nsp - 1)
    size = n // chunks
    late = chunks // 2

    def y_to(d):
        return lax.rem(t + 2 * d, ntp)

    def y_from(d):
        return lax.rem(t + ntp - 2 * d, ntp)

    def tp_to(d):
        return lax.rem(t + d, ntp)

    def tp_from(d):
        return lax.rem(t + ntp - d, ntp)

    barrier = pltpu.get_barrier_semaphore()
    for d in range(1, ntp):
        pl.semaphore_signal(barrier, inc=1, device_id=(s, tp_to(d)), device_id_type=MESH)
    pl.semaphore_signal(barrier, inc=1, device_id=(s_near, t), device_id_type=MESH)

    @pl.when(has_up)
    def _():
        pl.semaphore_signal(barrier, inc=1, device_id=(s_up, t), device_id_type=MESH)

    @pl.when(has_far)
    def _():
        pl.semaphore_signal(barrier, inc=1, device_id=(s_down, t), device_id_type=MESH)

    locals_in = []
    for k, (src, dst) in enumerate((
        (x_hbm, xg.at[t, pl.ds(n, n)]), (doc_hbm, doc_ref), (post_hbm, pg.at[t]), (ob_hbm, ob_ref), (pre_hbm, pre_ref),
    )):
        c = pltpu.make_async_copy(src, dst, loc_sem.at[k])
        c.start()
        locals_in.append(c)
    w_copies = []
    for l in range(LAYERS):
        for j, w in enumerate((wq_hbm, wk_hbm, wv_hbm, wo_hbm)):
            c = pltpu.make_async_copy(w.at[l], w_all.at[l, j], w_sem.at[l, j])
            c.start()
            w_copies.append(c)
    pl.semaphore_wait(barrier, ntp + has_up.astype(jnp.int32) + has_far.astype(jnp.int32))

    def remote(src, dst, ss, rs, dev):
        return pltpu.make_async_remote_copy(
            src_ref=src, dst_ref=dst, send_sem=ss, recv_sem=rs, device_id=dev, device_id_type=MESH
        )

    sends = []

    def run_if(cond, fn):
        if cond is None:
            fn()
        else:
            pl.when(cond)(fn)

    def go(c, cond=None):
        run_if(cond, c.start)
        sends.append((c, cond))

    def fire(c, cond=None):
        run_if(cond, c.start)

    def finish():
        for c, cond in sends:
            run_if(cond, c.wait_send)
        sends.clear()

    def drain(ref, sem, cond=None):
        run_if(cond, remote(ref, ref, sem, d_r.at[0], (s, partner)).wait_send)

    def drain_gather(g, buf):
        part = n - late * size
        for k in range(3):
            cond = has_far if k == far else None
            drain(buf.at[pl.ds(0, nc), pl.ds(0, n)], p_s.at[g, k], cond)
            drain(buf.at[pl.ds(0, nc - 1), pl.ds(0, n if k == own else late * size)], y_s.at[g, k], cond)
        for k, cond in ((0, None), (1, has_up)):
            drain(buf.at[0, pl.ds(0, n)], sp_s.at[g, k, 0], cond)
            drain(buf.at[pl.ds(0, nc - 1), pl.ds(0, part)], sp_s.at[g, k, 1], cond)

    def drain_att(l):
        drain(att.at[l, pl.ds(0, nc - 1)], ay_s.at[l])
        drain(att.at[l, pl.ds(0, nc)], ap_s.at[l])

    own, near, far = 0, 1, 2
    base_of = {own: n, near: near_row * n, far: far_row * n}
    u_base = (2 - near_row) * n

    def at(base, c):
        return pl.ds(pl.multiple_of(base + c * size, size), size)

    def p_send(g, buf, k, d, c, cond=None):
        blk = buf.at[y_from(d) if d else t, at(base_of[k], c)]
        fire(remote(blk, blk, p_s.at[g, k], p_r.at[g, k], (s, partner)), cond)

    def y_send(g, buf, k, c, cond=None):
        blk = buf.at[t, at(base_of[k], c)]
        for d in range(1, nc):
            fire(remote(blk, blk, y_s.at[g, k], y_r.at[g, k, d - 1, c], (s, y_to(d))), cond)

    def y_recv(g, buf, k, d, c, cond=None):
        blk = buf.at[y_from(d), at(base_of[k], c)]
        run_if(cond, remote(blk, blk, y_s.at[g, k], y_r.at[g, k, d - 1, c], (s, partner)).wait_recv)
        p_send(g, buf, k, d, c, cond)

    def near_send(g, buf, d, c):
        who = y_from(d) if d else t
        fire(
            remote(
                buf.at[who, at(n, c)], buf.at[who, at(u_base, c)],
                sp_s.at[g, 0, min(d, 1)], sp_r.at[g, 0, d, c], (s_near, t),
            )
        )

    def near_recv(g, buf, d, c):
        who = y_from(d) if d else t
        blk = buf.at[who, at(base_of[near], c)]
        remote(blk, blk, sp_s.at[g, 0, 0], sp_r.at[g, 0, d, c], (s, partner)).wait_recv()
        fire(
            remote(
                blk, buf.at[who, at(base_of[far], c)],
                sp_s.at[g, 1, min(d, 1)], sp_r.at[g, 1, d, c], (s_up, t),
            ),
            has_up,
        )
        if c < late:
            y_send(g, buf, near, c)
        p_send(g, buf, near, d, c)

    def far_recv(g, buf, d, c):
        who = y_from(d) if d else t
        blk = buf.at[who, at(base_of[far], c)]
        run_if(has_far, remote(blk, blk, sp_s.at[g, 1, 0], sp_r.at[g, 1, d, c], (s, partner)).wait_recv)
        if c < late:
            y_send(g, buf, far, c, has_far)
        p_send(g, buf, far, d, c, has_far)

    def own_recv(g, buf, d, c):
        y_recv(g, buf, own, d, c)
        if c >= late:
            near_send(g, buf, d, c)

    def start_own(g, buf):
        for c in list(range(late, chunks)) + list(range(late)):
            y_send(g, buf, own, c)
        for c in range(chunks):
            near_send(g, buf, 0, c)
        for c in range(chunks):
            p_send(g, buf, own, 0, c)

    def relay(g, buf):
        others = range(1, nc)
        for i in range(late):
            near_recv(g, buf, 0, i)
            for d in others:
                own_recv(g, buf, d, late + i)
        for i in range(late):
            near_recv(g, buf, 0, late + i)
            for d in others:
                own_recv(g, buf, d, i)
        for i in range(late):
            far_recv(g, buf, 0, i)
            for d in others:
                near_recv(g, buf, d, late + i)
                y_recv(g, buf, near, d, i)

    def relay_far(g, buf):
        others = range(1, nc)
        for i in range(late):
            far_recv(g, buf, 0, late + i)
        for i in range(late):
            for d in others:
                y_recv(g, buf, far, d, i, has_far)
                far_recv(g, buf, d, late + i)

    def wait_p(g, k, buf, cond=None):
        blk = buf.at[pl.ds(0, nc), pl.ds(0, n)]
        run_if(cond, remote(blk, blk, p_s.at[g, k], p_r.at[g, k], (s, partner)).wait_recv)

    for c in locals_in[:3]:
        c.wait()
    doc_near = remote(doc_ref, docs.at[0], d_s.at[0], d_r.at[0], (s_near, t))
    doc_far = remote(docs.at[0], docs.at[1], d_s.at[1], d_r.at[1], (s_up, t))
    go(doc_near)
    start_own(0, xg)
    for d in range(1, ntp):
        go(remote(pg.at[t], pg.at[t], g_s.at[d], g_r.at[d], (s, tp_to(d))))
    for c in locals_in[3:]:
        c.wait()

    span = fb.shape[2]
    for l in range(LAYERS):
        fb[l] = jnp.zeros_like(fb[l])
        for dr in range(2 * WIN_ROWS - 1):
            fb[l, :, dr * GRID_W:dr * GRID_W + 2 * WIN_COLS - 1] = ob_ref[l, dr]
    shift = span - ((WIN_ROWS - 1 - rim) * GRID_W + WIN_COLS - 1)

    def make_bias(i, _):
        line = jnp.broadcast_to(fb[i // heads, pl.ds(i % heads, 1), :], (n, span))
        bias[i] = pltpu.roll(line, shift, 1, stride=1, stride_axis=0)[:, :keys]
        return 0

    lax.fori_loop(0, heads, make_bias, 0)
    doc_near.wait_recv()
    go(doc_far, has_up)

    @pl.when(jnp.logical_not(has_far))
    def _():
        docs[1] = jnp.zeros_like(docs[1])
        rr = pl.ds(pl.multiple_of(far_row * n, n), n)
        kb[rr, :] = jnp.zeros((n, feat), BF16)
        vb[rr, :] = jnp.zeros((n, feat), BF16)

    own_docs = doc_ref[...].astype(F32)
    q_docs = jnp.transpose(jnp.broadcast_to(own_docs, (n, n)))
    qi = lax.broadcasted_iota(jnp.int32, (n, n), 0)
    ki = lax.broadcasted_iota(jnp.int32, (n, n), 1)
    all_rows = row_count * nsp
    q_row = s * row_count + qi // GRID_W
    q_col = qi % GRID_W
    a = jnp.clip(q_row - rim, 0, all_rows - WIN_ROWS)
    cs = jnp.clip(q_col - WIN_COLS // 2, 0, GRID_W - WIN_COLS)
    k_col = ki % GRID_W
    col_ok = (k_col >= cs) & (k_col < cs + WIN_COLS)
    relay(0, xg)
    run_if(has_far, doc_far.wait_recv)
    near_docs = docs[0].astype(F32)
    far_docs = docs[1].astype(F32)
    odd_f = odd.astype(F32)
    prev_docs = near_docs * odd_f + far_docs * (1.0 - odd_f)
    next_docs = far_docs * odd_f + near_docs * (1.0 - odd_f)
    for b, k_docs in enumerate((prev_docs, own_docs, next_docs)):
        k_row = (s + b - 1) * row_count + ki // GRID_W
        ok = (k_row >= a) & (k_row < a + WIN_ROWS) & col_ok
        ok = ok & (q_docs == jnp.broadcast_to(k_docs, (n, n)))
        mask[:, b * n:(b + 1) * n] = jnp.where(ok, 0.0, -jnp.inf)

    def qkv(l, k):
        r = pl.ds(pl.multiple_of(base_of[k], n), n)
        if l == 1:
            total = jnp.zeros((n, 1), F32)
            for j in range(ntp):
                br = bg[j, r, :].astype(F32)
                total = total + jnp.sum(br * br, axis=1, keepdims=True)
            scale = lax.rsqrt(total / width + EPS)
        stat = jnp.zeros((n, 1), F32)
        for j in range(ntp):
            xv = xg[j, r, :].astype(F32)
            if l == 1:
                br = bg[j, r, :].astype(F32)
                xn = (xv + br * scale * pg[j, 0:1, :]).astype(BF16)
                if k == own:
                    xg[j, r, :] = xn
                xv = xn.astype(F32)
            stat = stat + jnp.sum(xv * xv, axis=1, keepdims=True)
            xs[:, j * feat:(j + 1) * feat] = (xv * pre_ref[l:l + 1, j * feat:(j + 1) * feat]).astype(BF16)
        scaler = lax.rsqrt(stat / width + EPS)
        if k == own:
            qb[...] = (jnp.dot(xs[...], w_all[l, 0], preferred_element_type=F32) * scaler).astype(BF16)
        kb[r, :] = (jnp.dot(xs[...], w_all[l, 1], preferred_element_type=F32) * scaler).astype(BF16)
        vb[r, :] = (jnp.dot(xs[...], w_all[l, 2], preferred_element_type=F32) * scaler).astype(BF16)

    pw = 2 * HEAD_DIM
    lane = lax.broadcasted_iota(jnp.int32, (n, pw), 1)
    low = lane < HEAD_DIM
    score_scale = HEAD_DIM ** (-0.5)

    def attend(l, group):
        scs = []
        for p in group:
            q2 = qb[:, p * pw:(p + 1) * pw]
            k2 = kb[:, p * pw:(p + 1) * pw]
            for e in range(2):
                qe = jnp.where(low if e == 0 else ~low, q2, jnp.zeros_like(q2))
                sc = lax.dot_general(qe, k2, (((1,), (1,)), ((), ())), preferred_element_type=F32)
                scs.append(sc * score_scale + bias[l * heads + 2 * p + e] + mask[...])
        exs = [jnp.exp(sc - jnp.max(sc, axis=1, keepdims=True)) for sc in scs]
        for i, p in enumerate(group):
            v2 = vb[:, p * pw:(p + 1) * pw]
            outs = []
            for e in range(2):
                ex = exs[2 * i + e]
                o = jnp.dot(ex.astype(BF16), v2, preferred_element_type=F32)
                outs.append(o / jnp.sum(ex, axis=1, keepdims=True))
            att[l, t, p] = jnp.where(low, outs[0], outs[1]).astype(BF16)

    def send_att(l, p):
        blk = att.at[l, t, p]
        for d in range(1, nc):
            fire(remote(blk, blk, ay_s.at[l], ay_r.at[l, d - 1, p], (s, y_to(d))))
        fire(remote(blk, blk, ap_s.at[l], ap_r.at[l, 0], (s, partner)))

    def part_dot(l, who):
        wide = jnp.concatenate([att[l, who, p] for p in range(pairs)], axis=1)
        wrows = pl.ds(pl.multiple_of(who * feat, feat), feat)
        return jnp.dot(wide, w_all[l, 3, wrows, :], preferred_element_type=F32)

    def out_proj(l):
        acc = part_dot(l, t)
        for p in range(pairs):
            for d in range(1, nc):
                blk = att.at[l, y_from(d), p]
                remote(blk, blk, ay_s.at[l], ay_r.at[l, d - 1, p], (s, partner)).wait_recv()
                fire(remote(blk, blk, ap_s.at[l], ap_r.at[l, d], (s, partner)))
        for d in range(nc):
            who = lax.rem(partner + ntp - 2 * d, ntp)
            if d > 0:
                acc = acc + part_dot(l, y_from(d))
            blk = att.at[l, who]
            remote(blk, blk, ap_s.at[l], ap_r.at[l, d], (s, partner)).wait_recv()
            acc = acc + part_dot(l, who)
        return acc

    for l in range(LAYERS):
        buf = xg if l == 0 else bg
        if l == 1:
            relay(1, bg)
        wait_p(l, own, buf)
        for c in w_copies[4 * l:4 * l + 4]:
            c.wait()
        qkv(l, own)
        relay_far(l, buf)
        wait_p(l, near, buf)
        qkv(l, near)
        wait_p(l, far, buf, has_far)
        pl.when(has_far)(lambda l=l: qkv(l, far))
        for first in range(0, pairs, 2):
            group = list(range(first, min(first + 2, pairs)))
            attend(l, group)
            for p in group:
                send_att(l, p)
        branch = out_proj(l)
        if l == 0:
            bg[t, n:2 * n, :] = branch.astype(BF16)
            start_own(1, bg)
            finish()
            drain_gather(0, xg)
            drain_att(0)
            lax.fori_loop(heads, 2 * heads, make_bias, 0)
            for d in range(1, ntp):
                blk = pg.at[tp_from(d)]
                remote(blk, blk, g_s.at[d], g_r.at[d], (s, partner)).wait_recv()

    part = jnp.sum(branch * branch, axis=1, keepdims=True)
    flat = jnp.transpose(jnp.broadcast_to(part, (n, n)))[0:8, :]
    ssq[t] = flat
    for d in range(1, ntp):
        go(remote(ssq.at[t], ssq.at[t], q_s.at[d], q_r.at[d], (s, tp_to(d))))
    stream_ref[...] = xg[t, n:2 * n, :]
    for d in range(1, ntp):
        blk = ssq.at[tp_from(d)]
        remote(blk, blk, q_s.at[d], q_r.at[d], (s, partner)).wait_recv()
    total = ssq[0]
    for j in range(1, ntp):
        total = total + ssq[j]
    scale_row = lax.rsqrt(total[0:1, :] / width + EPS)
    scale = jnp.transpose(jnp.broadcast_to(scale_row, (n, n)))[:, 0:1]
    upd_ref[...] = branch * scale * pg[t, 1:2, :]
    finish()
    drain_gather(1, bg)
    drain_att(1)


def solution(mesh):
    nsp, ntp = mesh.shape["sp"], mesh.shape["tp"]

    def shards(grid_in, documents, pre_gain, wq, wk, wv, offset_bias, wo, post_gain):
        n, feat = grid_in.shape
        heads = offset_bias.shape[1]
        width = pre_gain.shape[1]
        span = 4 * n
        table = offset_bias.transpose(0, 2, 1, 3)
        chunks = n // GRID_W
        nc, pairs = ntp // 2, heads // 2
        dma = pltpu.SemaphoreType.DMA
        vm = pl.BlockSpec(memory_space=pltpu.VMEM)
        hb = pl.BlockSpec(memory_space=pltpu.HBM)
        update, stream = pl.pallas_call(
            functools.partial(kernel, nsp, ntp, heads, chunks),
            out_shape=(jax.ShapeDtypeStruct((n, feat), F32), jax.ShapeDtypeStruct((n, feat), BF16)),
            in_specs=[hb] * 9,
            out_specs=(vm, vm),
            scratch_shapes=[
                pltpu.VMEM((ntp, 3 * n, feat), BF16),
                pltpu.VMEM((ntp, 3 * n, feat), BF16),
                pltpu.VMEM((LAYERS, ntp, pairs, n, 2 * HEAD_DIM), BF16),
                pltpu.VMEM((2, 1, n), jnp.int32),
                pltpu.VMEM((ntp, LAYERS, feat), F32),
                pltpu.VMEM((ntp, 8, n), F32),
                pltpu.VMEM((LAYERS, 4, width, feat), BF16),
                pltpu.VMEM((n, width), BF16),
                pltpu.VMEM((n, feat), BF16),
                pltpu.VMEM((3 * n, feat), BF16),
                pltpu.VMEM((3 * n, feat), BF16),
                pltpu.VMEM((n, 3 * n), F32),
                pltpu.VMEM((LAYERS * heads, n, 3 * n), F32),
                pltpu.VMEM((LAYERS, heads, span), F32),
                pltpu.VMEM((1, n), jnp.int32),
                pltpu.VMEM((LAYERS, width), F32),
                pltpu.VMEM(table.shape, F32),
                dma((LAYERS, 4)),
                dma((5,)),
                dma((2, 2, 2)), dma((2, 2, nc, chunks)),
                dma((2, 3)), dma((2, 3, nc - 1, chunks)),
                dma((2, 3)), dma((2, 3)),
                dma((2,)), dma((2, nc - 1, pairs)),
                dma((2,)), dma((2, nc)),
                dma((2,)), dma((2,)),
                dma((ntp,)), dma((ntp,)),
                dma((ntp,)), dma((ntp,)),
            ],
            compiler_params=pltpu.CompilerParams(
                collective_id=0, has_side_effects=True, vmem_limit_bytes=58 * 1024 * 1024
            ),
        )(grid_in, documents.reshape(1, n), pre_gain, table, post_gain, wq, wk, wv, wo)
        return (stream.astype(F32) + update).astype(BF16)

    return jax.shard_map(
        shards,
        mesh=mesh,
        in_specs=(
            P("sp", "tp"),
            P("sp"),
            P(),
            P(None, None, "tp"),
            P(None, None, "tp"),
            P(None, None, "tp"),
            P(None, "tp", None, None),
            P(None, None, "tp"),
            P(None, "tp"),
        ),
        out_specs=P("sp", "tp"),
        check_vma=False,
    )
```

profile of v0, /device:TPU:3, one launch (start us, length us, event | category | flops | bytes accessed | tf_op | source)
XLA Modules:
  0.0 48.7 jit_solution(1398620271389532272)
XLA Ops:
  0.0 47.1 %shard_map.91 = (f32[128,512]{1,0:T(8,128)}, bf16[128,512]{1,0:T(8,128)(2,1)}) custom-call(bf16[128,512]{1,0:T(8,128)(2,1)} %x_hbm.1, s32[1,128]{1,0:T(1,128)} %bitcast.3, f32[2,2048]{1,0:T(2,128)} %pre_hbm.1, f32[2,15,8,31]{3,2,1,0:T(8,128)} %bitcast.2, f32[2,512]{1,0:T(2,128)} %post_hbm.1, bf16[2,2048,512]{2,1,0:T(8,128)(2,1)} %wq_hbm.1, ...), custom_call_target="tpu_custom_call" | custom-call | tf_op jit(solution)/shard_map/pallas_call | solution.py:427
  47.1 1.7 %add_convert_fusion = bf16[128,512]{1,0:T(8,128)(2,1)} fusion(f32[128,512]{1,0:T(8,128)} %get-tuple-element.8, bf16[128,512]{1,0:T(8,128)(2,1)} %get-tuple-element.7), kind=kLoop, calls=%fused_computation | loop fusion | flops 196608 | bytes 524288 | tf_op jit(solution)/shard_map/convert_element_type | solution.py:465
where the time goes:
time: 49 us; the launch traced here: 48.7 us
  Pallas kernels  47.1 us (96%)
  other arithmetic  1.67 us (3%)
    pallas_call x1, Pallas kernels, shards(): pl.pallas_call(functools.partial(kernel, nsp, ntp, heads, chunks), out_sh...  47.1 us
    convert_element_type x1, other arithmetic, shards(): return (stream.astype(F32) + update).astype(BF16)  1.67 us

commit v1 on v0

--- a/solution.py
+++ b/solution.py
@@ -20,7 +20,7 @@
 
 def kernel(
     nsp, ntp, heads, chunks, x_hbm, doc_hbm, pre_hbm, ob_hbm, post_hbm, wq_hbm, wk_hbm, wv_hbm, wo_hbm,
-    upd_ref, stream_ref,
+    out_ref,
     xg, bg, att, docs, pg, ssq, w_all, xs, qb, kb, vb, mask, bias, fb, doc_ref, pre_ref, ob_ref,
     w_sem, loc_sem, sp_s, sp_r, y_s, y_r, p_s, p_r, ay_s, ay_r, ap_s, ap_r, d_s, d_r, g_s, g_r, q_s, q_r,
 ):
@@ -81,12 +81,6 @@
         c = pltpu.make_async_copy(src, dst, loc_sem.at[k])
         c.start()
         locals_in.append(c)
-    w_copies = []
-    for l in range(LAYERS):
-        for j, w in enumerate((wq_hbm, wk_hbm, wv_hbm, wo_hbm)):
-            c = pltpu.make_async_copy(w.at[l], w_all.at[l, j], w_sem.at[l, j])
-            c.start()
-            w_copies.append(c)
     pl.semaphore_wait(barrier, ntp + has_up.astype(jnp.int32) + has_far.astype(jnp.int32))
 
     def remote(src, dst, ss, rs, dev):
@@ -226,12 +220,19 @@
         blk = buf.at[pl.ds(0, nc), pl.ds(0, n)]
         run_if(cond, remote(blk, blk, p_s.at[g, k], p_r.at[g, k], (s, partner)).wait_recv)
 
-    for c in locals_in[:3]:
-        c.wait()
+    locals_in[0].wait()
+    locals_in[1].wait()
+    locals_in[2].wait()
     doc_near = remote(doc_ref, docs.at[0], d_s.at[0], d_r.at[0], (s_near, t))
     doc_far = remote(docs.at[0], docs.at[1], d_s.at[1], d_r.at[1], (s_up, t))
     go(doc_near)
     start_own(0, xg)
+    w_copies = []
+    for l in range(LAYERS):
+        for j, w in enumerate((wq_hbm, wk_hbm, wv_hbm, wo_hbm)):
+            c = pltpu.make_async_copy(w.at[l], w_all.at[l, j], w_sem.at[l, j])
+            c.start()
+            w_copies.append(c)
     for d in range(1, ntp):
         go(remote(pg.at[t], pg.at[t], g_s.at[d], g_r.at[d], (s, tp_to(d))))
     for c in locals_in[3:]:
@@ -395,7 +396,6 @@
     ssq[t] = flat
     for d in range(1, ntp):
         go(remote(ssq.at[t], ssq.at[t], q_s.at[d], q_r.at[d], (s, tp_to(d))))
-    stream_ref[...] = xg[t, n:2 * n, :]
     for d in range(1, ntp):
         blk = ssq.at[tp_from(d)]
         remote(blk, blk, q_s.at[d], q_r.at[d], (s, partner)).wait_recv()
@@ -404,7 +404,7 @@
         total = total + ssq[j]
     scale_row = lax.rsqrt(total[0:1, :] / width + EPS)
     scale = jnp.transpose(jnp.broadcast_to(scale_row, (n, n)))[:, 0:1]
-    upd_ref[...] = branch * scale * pg[t, 1:2, :]
+    out_ref[...] = (xg[t, n:2 * n, :].astype(F32) + branch * scale * pg[t, 1:2, :]).astype(BF16)
     finish()
     drain_gather(1, bg)
     drain_att(1)
@@ -424,11 +424,11 @@
         dma = pltpu.SemaphoreType.DMA
         vm = pl.BlockSpec(memory_space=pltpu.VMEM)
         hb = pl.BlockSpec(memory_space=pltpu.HBM)
-        update, stream = pl.pallas_call(
+        return pl.pallas_call(
             functools.partial(kernel, nsp, ntp, heads, chunks),
-            out_shape=(jax.ShapeDtypeStruct((n, feat), F32), jax.ShapeDtypeStruct((n, feat), BF16)),
+            out_shape=pltpu.VMEM((n, feat), BF16),
             in_specs=[hb] * 9,
-            out_specs=(vm, vm),
+            out_specs=vm,
             scratch_shapes=[
                 pltpu.VMEM((ntp, 3 * n, feat), BF16),
                 pltpu.VMEM((ntp, 3 * n, feat), BF16),
@@ -462,7 +462,6 @@
                 collective_id=0, has_side_effects=True, vmem_limit_bytes=58 * 1024 * 1024
             ),
         )(grid_in, documents.reshape(1, n), pre_gain, table, post_gain, wq, wk, wv, wo)
-        return (stream.astype(F32) + update).astype(BF16)
 
     return jax.shard_map(
         shards,

time: 49 us -> 44.1 us (0.900)
  Pallas kernels: 47.1 us -> 43.2 us
  other arithmetic: 1.67 us -> 0 us
  local copies, waits for them, and re-layouts: 0 us -> 0.66 us
    pallas_call x1, Pallas kernels: 47.1 us -> 43.2 us  [shards(): pl.pallas_call(functools.partial(kernel, nsp, ntp, heads, chunks), out_sh...]
    convert_element_type x1 -> x0, other arithmetic: 1.67 us -> none  [shards(): return (stream.astype(F32) + update).astype(BF16)]
    unnamed x0 -> x1, local copies, waits for them, and re-layouts: none -> 0.66 us
where the time goes in v1:
time: 44.1 us; the launch traced here: 43.9 us
  Pallas kernels  43.2 us (98%)
  local copies, waits for them, and re-layouts  0.66 us (1%)
    pallas_call x1, Pallas kernels, shards(): pl.pallas_call(functools.partial(kernel, nsp, ntp, heads, chunks), out_sh...  43.2 us

profile of v1, /device:TPU:3, one launch (start us, length us, event | category | flops | bytes accessed | tf_op | source)
XLA Modules:
  0.0 43.9 jit_solution(8189006834115309958)
XLA Ops:
  0.0 43.2 %shard_map.91 = bf16[128,512]{1,0:T(8,128)(2,1)S(1)} custom-call(bf16[128,512]{1,0:T(8,128)(2,1)} %x_hbm.1, s32[1,128]{1,0:T(1,128)} %bitcast.3, f32[2,2048]{1,0:T(2,128)} %pre_hbm.1, f32[2,15,8,31]{3,2,1,0:T(8,128)} %bitcast.2, f32[2,512]{1,0:T(2,128)} %post_hbm.1, bf16[2,2048,512]{2,1,0:T(8,128)(2,1)} %wq_hbm.1, bf16[2,2048,512]{2,1,0:T(8,128)(2,1)} %wk_hbm.1, ...), custom_call_target="tpu_custom_call" | custom-call | tf_op jit(solution)/shard_map/pallas_call | solution.py:427
  43.3 0.7 %copy.11 = bf16[128,512]{1,0:T(8,128)(2,1)} copy(bf16[128,512]{1,0:T(8,128)(2,1)S(1)} %shard_map.91) | data formatting | bytes 262144
